TPU v7x, 512 devices: a whole 4x8x8 slice. The times are simulated.
512 devices in a mesh: ep: 32 (over z, x), tp: 16 (over y, core).
Axes of the slice: x: 4, y: 8, z: 8, core: 2. Of those that a mesh axis runs over, the one named last changes fastest.
Arguments:
- conv_value: bfloat16 [16384, 2048], P('ep', 'tp'), may hold values from -6 to 6
- conv_gate: bfloat16 [16384, 2048], P('ep', 'tp'), may hold values from -9 to 9
- conv_taps: float32 [31, 2048], P(None, 'tp'), may hold values from -14 to 14
- norm_gain: float32 [2048], P('tp'), may hold values from 0.1 to 1.9
- norm_shift: float32 [2048], P('tp'), may hold values from -3 to 3
- conv_out_weight: bfloat16 [2048, 2048], P(None, 'tp'), may hold values from -0.125 to 0.125
- moe_input: bfloat16 [4096, 2048], P('ep'), may hold values from -6 to 6
- moe_gain: float32 [2048], replicated, may hold values from 0.1 to 1.9
- routes: int32 [4096, 4], P('ep'), may hold values from 0 to 31, all different within a row; in each aligned block of 128 rows (0 to 127, 128 to 255, ...) at most 32 rows name the same one
- route_weights: float32 [4096, 4], P('ep'), may hold values from 0.25 to 1
- expert_gate: bfloat16 [32, 2048, 4096], P('ep', None, 'tp'), may hold values from -0.125 to 0.125
- expert_up: bfloat16 [32, 2048, 4096], P('ep', None, 'tp'), may hold values from -0.125 to 0.125
- expert_down: bfloat16 [32, 4096, 2048], P('ep', None, 'tp'), may hold values from -0.09375 to 0.09375
- shared_gate: bfloat16 [2048, 512], P(None, 'tp'), may hold values from -0.125 to 0.125
- shared_up: bfloat16 [2048, 512], P(None, 'tp'), may hold values from -0.125 to 0.125
- shared_down: bfloat16 [512, 2048], P(None, 'tp'), may hold values from -0.25 to 0.25
Outputs:
- conv_result: bfloat16 [16384, 2048], P('ep', 'tp')
- moe_result: bfloat16 [4096, 2048], P('ep', 'tp')
Inputs may be any that keep to these rules, and one draw needn't show every extreme that they name: `routes`: in the rows of one device (aligned blocks of 128 rows) no expert is named by more than 32 rows, a bound that some block reaches; each row names 4 different experts.
All inputs are finite; a program needn't handle non-finite values.
Results may differ from a plain program's by a relative error of at most 0.0068.
Values may be sent and summed in bfloat16 or wider, within the bound.
A program may use at most 64 MiB of HBM per device.

v0:
```python
import jax
import jax.numpy as jnp
from jax import lax
from jax.sharding import Mesh
from jax.sharding import PartitionSpec as P

EP = ("ep_0", "ep_1")


def from_behind(value, axis, steps):
    count = lax.axis_size(axis)
    initial, last = (max(0, -steps), min(count, count - steps))
    return lax.ppermute(value, axis, [(source, source + steps) for source in range(initial, last)])


def cut_along(array, dim, peers):
    before, after = (array.shape[:dim], array.shape[dim + 1 :])
    return jnp.moveaxis(array.reshape(*before, peers, -1, *after), dim, 0)


def joined_along(parts, dim):
    lengths = list(parts.shape[1:])
    lengths[dim] *= parts.shape[0]
    return jnp.moveaxis(parts, 0, dim).reshape(lengths)


def exchange_in_order(parts, axes, turns):
    lengths = [lax.axis_size(a) for a in axes]
    parts = parts.reshape(*lengths, *parts.shape[1:])
    for k in turns:
        parts = lax.all_to_all(parts, axes[k], split_axis=k, concat_axis=k, tiled=True)
    return parts.reshape(-1, *parts.shape[len(axes) :])


def stepwise_exchange(array, axes, turns, split_dim, concat_dim):
    parts = cut_along(array, split_dim, lax.axis_size(axes))
    return joined_along(exchange_in_order(parts, axes, turns), concat_dim)


def body(
    conv_value,
    conv_gate,
    conv_taps,
    norm_gain,
    norm_shift,
    conv_out_weight,
    moe_input,
    moe_gain,
    routes,
    route_weights,
    expert_gate,
    expert_up,
    expert_down,
    shared_gate,
    shared_up,
    shared_down,
):
    tap_count = conv_taps.shape[0]
    rows_a = conv_value.shape[0]
    glu_rows = (
        conv_value.astype(jnp.float32) * jax.nn.sigmoid(conv_gate.astype(jnp.float32))
    ).astype(jnp.bfloat16)
    before = from_behind(glu_rows[rows_a - (tap_count - 1) :], EP, 1)
    padded = jnp.concatenate([before, glu_rows], axis=0)
    filtered = jnp.zeros(glu_rows.shape, jnp.float32)
    for offset in range(tap_count):
        filtered = filtered + conv_taps[offset] * padded[offset : offset + rows_a].astype(
            jnp.float32
        )
    row_total, squares = lax.psum(
        (jnp.sum(filtered, axis=1), jnp.sum(filtered * filtered, axis=1)), "tp"
    )
    channels = conv_out_weight.shape[0]
    row_mean = row_total / channels
    row_square = squares / channels
    scaled = (filtered - row_mean[:, None]) * lax.rsqrt(row_square - row_mean * row_mean + 1e-05)[
        :, None
    ]
    conv_hidden = jax.nn.silu(scaled * norm_gain + norm_shift).astype(jnp.bfloat16)
    conv_sum = jnp.dot(
        lax.all_gather(conv_hidden, "tp", axis=1, tiled=True),
        conv_out_weight,
        preferred_element_type=jnp.float32,
    )
    conv_result = conv_sum.astype(jnp.bfloat16)
    inputs = moe_input.astype(jnp.float32)
    normed = (
        inputs * lax.rsqrt(jnp.mean(inputs * inputs, axis=1, keepdims=True) + 1e-06) * moe_gain
    ).astype(jnp.bfloat16)
    rows_b, per_row = routes.shape
    model_width = normed.shape[1]
    groups = lax.axis_size(EP)
    capacity = 2 * rows_b * per_row // groups
    flat_expert = routes.reshape(-1)
    owner_row = jnp.arange(rows_b * per_row, dtype=jnp.int32) // per_row
    expert_hits = (flat_expert[:, None] == jnp.arange(groups, dtype=jnp.int32)[None, :]).astype(
        jnp.int32
    )
    slot_rank = jnp.sum((jnp.cumsum(expert_hits, axis=0) - expert_hits) * expert_hits, axis=1)
    slot_index = flat_expert * capacity + slot_rank
    outgoing = (
        jnp.zeros((groups * capacity, model_width), jnp.bfloat16)
        .at[slot_index]
        .set(normed[owner_row])
    )
    outgoing = outgoing.reshape(groups, capacity, model_width)
    slot_share = capacity // lax.axis_size("tp")
    own_slots = lax.dynamic_slice_in_dim(outgoing, lax.axis_index("tp") * slot_share, slot_share, 1)
    partial_rows = lax.all_to_all(own_slots, EP, split_axis=0, concat_axis=0, tiled=True)
    arrived = lax.all_gather(partial_rows, "tp", axis=1, tiled=True)
    arrived_rows = arrived.reshape(groups * capacity, model_width)
    gate_value = jnp.dot(arrived_rows, expert_gate[0], preferred_element_type=jnp.float32)
    upward = jnp.dot(arrived_rows, expert_up[0], preferred_element_type=jnp.float32)
    expert_hidden = (jax.nn.silu(gate_value) * upward).astype(jnp.bfloat16)
    shared_hidden = (
        jax.nn.silu(jnp.dot(normed, shared_gate, preferred_element_type=jnp.float32))
        * jnp.dot(normed, shared_up, preferred_element_type=jnp.float32)
    ).astype(jnp.bfloat16)
    columns = expert_down.shape[2]
    routed_rows = expert_down[0]
    routed_sum = jnp.dot(
        lax.all_gather(expert_hidden, "tp", axis=1, tiled=True),
        routed_rows,
        preferred_element_type=jnp.float32,
    )
    shared_sum = jnp.dot(
        lax.all_gather(shared_hidden, "tp", axis=1, tiled=True),
        shared_down,
        preferred_element_type=jnp.float32,
    )
    expert_out = routed_sum.astype(jnp.bfloat16).reshape(groups, capacity, columns)
    returned = stepwise_exchange(expert_out, EP, (0, 1), 0, 0).reshape(groups * capacity, columns)
    picked = returned[slot_index].astype(jnp.float32) * route_weights.reshape(-1)[:, None]
    moe_sum = jnp.sum(picked.reshape(rows_b, per_row, columns), axis=1) + shared_sum
    return (conv_result, moe_sum.astype(jnp.bfloat16))


def solution(mesh):
    finer = Mesh(mesh.devices.reshape(8, 4, mesh.shape["tp"]), ("ep_0", "ep_1", "tp"))
    in_specs = (
        P(EP, "tp"),
        P(EP, "tp"),
        P(None, "tp"),
        P("tp"),
        P("tp"),
        P(None, "tp"),
        P(EP, None),
        P(),
        P(EP, None),
        P(EP, None),
        P(EP, None, "tp"),
        P(EP, None, "tp"),
        P(EP, None, "tp"),
        P(None, "tp"),
        P(None, "tp"),
        P(None, "tp"),
    )
    out_specs = (P(EP, "tp"), P(EP, "tp"))
    return jax.shard_map(body, mesh=finer, in_specs=in_specs, out_specs=out_specs, check_vma=False)
```

profile of v0, /device:TPU:1, one launch (start us, length us, event | category | flops | bytes accessed | tf_op | source)
XLA Modules:
  0.0 226.3 jit_solution(18367188397835349781)
XLA Ops:
  7.2 0.0 copy-start
  7.2 0.0 all-gather.6.cloned.1.call-start
  7.2 0.8 broadcast_multiply_fusion
  8.0 0.8 copy.33
  8.8 0.1 eq.29
  8.9 0.1 eq.25
  9.0 1.2 fusion.6
  10.3 0.1 copy.32
  10.4 0.1 mul.506
  10.5 1.2 reduce-window.6
  11.7 0.2 slice_reduce_fusion
  11.9 0.1 fusion.45
  12.1 1.2 fusion.8
  13.3 12.8 %scatter_custom_fusion = bf16[1024,2048]{1,0:T(8,128)(2,1)} fusion(s32[512]{0:T(512)S(1)} %bitcast.118, bf16[128,2048]{1,0:T(8,128)(2,1)S(1)} %fusion.8, s32[1024]{0:T(1024)S(1)} %pad_clamp_fusion.1, bf16[]{:T(256)} %constant.47.clone.1), kind=kCustom, calls=%fused_computation.3 | custom fusion | bytes 4194306 | tf_op jit(solution)/shard_map/scatter | solution.py:104
  26.1 1.5 constant_dynamic-slice_fusion
  27.6 24.8 %all_to_all.15 = bf16[32,2,2048]{2,1,0:T(2,128)(2,1)S(1)} all-to-all(bf16[32,2,2048]{2,1,0:T(2,128)(2,1)S(1)} %constant_dynamic-slice_fusion), channel_id=1, replica_groups=mesh['ep_0'=8,'ep_1'=4,'tp'=16] {'ep_0','ep_1'}, dimensions={0} | all-to-all | bytes 524288 | tf_op jit(solution)/shard_map/all_to_all | solution.py:109
  52.4 0.8 copy.36
  53.2 0.0 all-gather.6.cloned.1.call-update
  53.2 0.0 all-gather.8.cloned.1.call-start
  53.3 42.1 %all-gather.6.cloned.1.call-done = bf16[32,32,2048]{2,0,1:T(8,128)(2,1)} async-done(((bf16[32,2,2048]{2,0,1:T(8,128)(2,1)}), bf16[32,32,2048]{2,0,1:T(8,128)(2,1)}) %all-gather.6.cloned.1.call-update) | async-done | bytes 4194320 | tf_op jit(solution)/shard_map/all_gather | solution.py:110
  95.4 4.5 %copy.37 = bf16[32,32,2048]{2,1,0:T(8,128)(2,1)S(1)} copy(bf16[32,32,2048]{2,0,1:T(8,128)(2,1)} %all-gather.6.cloned.1.call-done) | data formatting | bytes 8388608 | tf_op jit(solution)/shard_map/all_gather | solution.py:110
  99.9 1.3 fusion.11
  101.2 0.0 copy-start.2
  101.2 2.1 fusion.3
  103.4 0.0 all-gather.8.cloned.1.call-update
  103.4 0.0 all-gather.4.cloned.1.call-start
  103.4 0.1 multiply_convert_fusion.1
  103.5 3.1 %collective-permute-start = (bf16[30,128]{1,0:T(8,128)(2,1)S(1)}, bf16[30,128]{1,0:T(8,128)(2,1)S(1)}, u32[]{:S(2)}, u32[]{:S(2)}) collective-permute-start(bf16[30,128]{1,0:T(8,128)(2,1)S(1)} %slice.260), channel_id=1, source_target_pairs={{0,16},{16,32},{32,48},{48,64},{64,80},{80,96},{96,112},{112,128},... | collective-permute-start | bytes 23048 | tf_op jit(solution)/shard_map/ppermute | solution.py:13
  106.7 0.7 collective-permute-done
  107.4 1.2 fusion.47
  108.6 25.0 %all-reduce = (f32[512]{0:T(512)S(1)}, f32[512]{0:T(512)S(1)}) all-reduce(f32[512]{0:T(512)S(1)} %get-tuple-element.3, f32[512]{0:T(512)S(1)} %get-tuple-element.2), channel_id=1, replica_groups=mesh['ep_0'=8,'ep_1'=4,'tp'=16] {'tp'}, use_global_device_ids=true, to_apply=%region_3.0 | all-reduce | flops 1024 | bytes 8192 | tf_op jit(solution)/shard_map/psum | solution.py:70
  133.7 0.9 multiply_convert_fusion
  134.5 0.0 all-gather.4.cloned.1.call-update
  134.6 35.8 %all-gather.8.cloned.1.call-done = bf16[1024,4096]{1,0:T(8,128)(2,1)} async-done(((bf16[1024,256]{1,0:T(8,128)(2,1)}), bf16[1024,4096]{1,0:T(8,128)(2,1)}) %all-gather.8.cloned.1.call-update) | async-done | bytes 8388624 | tf_op jit(solution)/shard_map/all_gather | solution.py:122
  170.4 6.7 %convolution_convert_fusion = bf16[1024,128]{1,0:T(8,128)(2,1)} fusion(bf16[1024,4096]{1,0:T(8,128)(2,1)} %all-gather.8.cloned.1.call-done, bf16[1,4096,128]{2,1,0:T(8,128)(2,1)} %param.28), kind=kOutput, calls=%fused_computation.39 | convolution fusion | flops 1073872896 | bytes 9699328 | tf_op jit(solution)/shard_map/dot_general | solution.py:121
  177.1 6.5 %all-to-all-start.1 = ((bf16[8,4,1,32,128]{4,3,1,2,0:T(8,128)(2,1)}), bf16[8,4,1,32,128]{4,3,1,2,0:T(8,128)(2,1)S(1)}, u32[]{:S(2)}, u32[]{:S(2)}) async-start(bf16[8,4,1,32,128]{4,3,1,2,0:T(8,128)(2,1)} %bitcast.41), calls=%async_computation.1 | async-start | bytes 524288 | tf_op jit(solution)/shard_map/all_to_all | solution.py:31
  183.6 0.3 fusion.48
  183.9 0.0 copy-done.8
  183.9 0.1 copy.41
  184.1 0.3 fusion.5
  184.3 16.1 %all_gather.15 = bf16[128,512]{0,1:T(8,128)(2,1)S(1)} all-gather(bf16[128,32]{0,1:T(8,128)(2,1)S(1)} %fusion.5), channel_id=1, replica_groups=mesh['ep_0'=8,'ep_1'=4,'tp'=16] {'tp'}, dimensions={1}, use_global_device_ids=true | all-gather | bytes 139264 | tf_op jit(solution)/shard_map/all_gather | solution.py:127
  200.4 0.7 copy.39
  201.1 4.1 %all-to-all-start.2 = ((bf16[8,4,1,32,128]{4,3,0,2,1:T(8,128)(2,1)}), bf16[8,4,1,32,128]{4,3,0,2,1:T(8,128)(2,1)S(1)}, u32[]{:S(2)}, u32[]{:S(2)}) async-start(bf16[8,4,1,32,128]{4,3,0,2,1:T(8,128)(2,1)} %copy.39), calls=%async_computation.2 | async-start | bytes 524288 | tf_op jit(solution)/shard_map/all_to_all | solution.py:31
  205.2 9.1 %all-gather.4.cloned.1.call-done = bf16[512,2048]{1,0:T(8,128)(2,1)} async-done(((bf16[512,128]{1,0:T(8,128)(2,1)}), bf16[512,2048]{1,0:T(8,128)(2,1)}) %all-gather.4.cloned.1.call-update) | async-done | bytes 2097168 | tf_op jit(solution)/shard_map/all_gather | solution.py:81
  214.3 3.0 %convolution_convert_fusion.1 = bf16[512,128]{1,0:T(8,128)(2,1)} fusion(bf16[512,2048]{1,0:T(8,128)(2,1)} %all-gather.4.cloned.1.call-done, bf16[2048,128]{1,0:T(8,128)(2,1)S(1)} %copy-done.1), kind=kOutput, calls=%fused_computation.40 | convolution fusion | flops 268500992 | bytes 2752512 | tf_op jit(solution)/shard_map/dot_general | solution.py:80
  217.3 1.3 gather_fusion
  218.6 0.2 fusion.13
  218.9 0.8 fusion.4
  (36 shorter events, 0.2 us)
Async XLA Ops:
  7.2 92.7 %copy-start = (bf16[1,2048,256]{2,1,0:T(8,128)(2,1)S(1)}, bf16[1,2048,256]{2,1,0:T(8,128)(2,1)}, u32[]{:S(2)}) copy-start(bf16[1,2048,256]{2,1,0:T(8,128)(2,1)} %param.26) | copy-start | bytes 3145732
  7.2 88.2 %all-gather.6.cloned.1.call-start = ((), (), s32[]{:S(2)}) async-start(), calls=%async_computation.4 | async-start | bytes 4456448 | tf_op jit(solution)/shard_map/all_gather | solution.py:110
  53.2 117.2 %all-gather.8.cloned.1.call-start = ((), (), s32[]{:S(2)}) async-start(), calls=%async_computation.5 | async-start | bytes 8912896 | tf_op jit(solution)/shard_map/all_gather | solution.py:122
  99.9 1.3 copy-start.11
  101.2 2.3 copy-start.2
  101.2 2.3 copy-start.3
  101.2 5.5 %copy-start.7 = (f32[31,128]{1,0:T(8,128)S(1)}, f32[31,128]{1,0:T(8,128)}, u32[]{:S(2)}) copy-start(f32[31,128]{1,0:T(8,128)} %param.18) | copy-start | bytes 47620
  101.2 32.4 %copy-start.9 = (f32[128]{0:T(128)S(1)}, f32[128]{0:T(128)}, u32[]{:S(2)}) copy-start(f32[128]{0:T(128)} %param.20) | copy-start | bytes 1540
  101.2 32.4 %copy-start.10 = (f32[128]{0:T(128)S(1)}, f32[128]{0:T(128)}, u32[]{:S(2)}) copy-start(f32[128]{0:T(128)} %param.19) | copy-start | bytes 1540
  103.4 110.9 %all-gather.4.cloned.1.call-start = ((), (), s32[]{:S(2)}) async-start(), calls=%async_computation.3 | async-start | bytes 2228224 | tf_op jit(solution)/shard_map/all_gather | solution.py:81
  103.5 3.9 %collective-permute-start = (bf16[30,128]{1,0:T(8,128)(2,1)S(1)}, bf16[30,128]{1,0:T(8,128)(2,1)S(1)}, u32[]{:S(2)}, u32[]{:S(2)}) collective-permute-start(bf16[30,128]{1,0:T(8,128)(2,1)S(1)} %slice.260), channel_id=1, source_target_pairs={{0,16},{16,32},{32,48},{48,64},{64,80},{80,96},{96,112},{112,128},... | collective-permute-start | bytes 23048 | tf_op jit(solution)/shard_map/ppermute | solution.py:13
  134.6 49.1 %copy-start.4 = (bf16[2048,32]{0,1:T(8,128)(2,1)S(1)}, bf16[2048,32]{0,1:T(8,128)(2,1)}, u32[]{:S(2)}) copy-start(bf16[2048,32]{0,1:T(8,128)(2,1)} %param.29) | copy-start | bytes 393220
  134.6 49.3 %copy-start.8 = (f32[128,4]{0,1:T(4,128)S(1)}, f32[128,4]{0,1:T(4,128)}, u32[]{:S(2)}) copy-start(f32[128,4]{0,1:T(4,128)} %param.25) | copy-start | bytes 6148
  134.6 49.5 %copy-start.5 = (bf16[2048,32]{0,1:T(8,128)(2,1)S(1)}, bf16[2048,32]{0,1:T(8,128)(2,1)}, u32[]{:S(2)}) copy-start(bf16[2048,32]{0,1:T(8,128)(2,1)} %param.30) | copy-start | bytes 393220
  134.6 79.7 %copy-start.1 = (bf16[2048,128]{1,0:T(8,128)(2,1)S(1)}, bf16[2048,128]{1,0:T(8,128)(2,1)}, u32[]{:S(2)}) copy-start(bf16[2048,128]{1,0:T(8,128)(2,1)} %param.21) | copy-start | bytes 1572868
  177.1 41.8 %copy-start.6 = (bf16[512,128]{1,0:T(8,128)(2,1)S(1)}, bf16[512,128]{1,0:T(8,128)(2,1)}, u32[]{:S(2)}) copy-start(bf16[512,128]{1,0:T(8,128)(2,1)} %param.31) | copy-start | bytes 393220
  177.1 23.3 %all-to-all-start.1 = ((bf16[8,4,1,32,128]{4,3,1,2,0:T(8,128)(2,1)}), bf16[8,4,1,32,128]{4,3,1,2,0:T(8,128)(2,1)S(1)}, u32[]{:S(2)}, u32[]{:S(2)}) async-start(bf16[8,4,1,32,128]{4,3,1,2,0:T(8,128)(2,1)} %bitcast.41), calls=%async_computation.1 | async-start | bytes 524288 | tf_op jit(solution)/shard_map/all_to_all | solution.py:31
  201.1 16.1 %all-to-all-start.2 = ((bf16[8,4,1,32,128]{4,3,0,2,1:T(8,128)(2,1)}), bf16[8,4,1,32,128]{4,3,0,2,1:T(8,128)(2,1)S(1)}, u32[]{:S(2)}, u32[]{:S(2)}) async-start(bf16[8,4,1,32,128]{4,3,0,2,1:T(8,128)(2,1)} %copy.39), calls=%async_computation.2 | async-start | bytes 524288 | tf_op jit(solution)/shard_map/all_to_all | solution.py:31
Sparse Core Ops, SparseCore 0:
  53.3 42.0 all-gather.5
  103.5 66.8 all-gather.7
  173.1 41.1 all-gather.3
where the time goes:
time: 227 us; the launch traced here: 226 us
  waiting for transfers between devices  87.8 us (39%)
  blocking collectives  65.9 us (29%)
  local copies, waits for them, and re-layouts  23.3 us (10%)
  matrix products  14.4 us (6%)
  between operations  14 us (6%)
  starting transfers between devices  13.8 us (6%)
  other arithmetic  6.99 us (3%)
    all_gather x1, waiting for transfers between devices, body(): arrived = lax.all_gather(partial_rows, 'tp', axis=1, tiled=True)  42.1 us
    all_gather x1, waiting for transfers between devices, body(): lax.all_gather(expert_hidden, 'tp', axis=1, tiled=True)  35.8 us
    psum x1, blocking collectives, body(): lax.psum((jnp.sum(filtered, axis=1), jnp.sum(filtered * filtered, axis=1)...  25 us
    all_to_all x1, blocking collectives, body(): lax.all_to_all(own_slots, EP, split_axis=0, concat_axis=0, tiled=True)  24.8 us
    all_gather x1, blocking collectives, body(): lax.all_gather(shared_hidden, 'tp', axis=1, tiled=True)  16.1 us
    scatter x1, local copies, waits for them, and re-layouts, body(): outgoing = jnp.zeros((groups * capacity, model_width), jnp.bfloat16).at[s...  12.8 us
    all_to_all x2, starting transfers between devices, exchange_in_order(): lax.all_to_all(parts, axes[k], split_axis=k, concat_axis=k, tiled=True)  10.6 us
    all_gather x1, waiting for transfers between devices, body(): lax.all_gather(conv_hidden, 'tp', axis=1, tiled=True)  9.08 us
  transfers between devices with their start and end apart: 6, of which 4 were waited for; matrix products, arithmetic and copies ran while one was open for 6% of the time, Pallas kernels for 0%

commit v1 on v0

--- a/solution.py
+++ b/solution.py
@@ -118,10 +118,17 @@
     ).astype(jnp.bfloat16)
     columns = expert_down.shape[2]
     routed_rows = expert_down[0]
+    trails_bring = lambda s0: jnp.concatenate(
+        lax.all_to_all(
+            jnp.stack([s0 for _ in range(lax.psum(1, axis_name="tp"))]),
+            concat_axis=0,
+            split_axis=0,
+            axis_name="tp",
+        ),
+        axis=1,
+    )
     routed_sum = jnp.dot(
-        lax.all_gather(expert_hidden, "tp", axis=1, tiled=True),
-        routed_rows,
-        preferred_element_type=jnp.float32,
+        trails_bring(expert_hidden), routed_rows, preferred_element_type=jnp.float32
     )
     shared_sum = jnp.dot(
         lax.all_gather(shared_hidden, "tp", axis=1, tiled=True),

time: 227 us -> 373 us (1.64)
  blocking collectives: 65.9 us -> 237 us
  waiting for transfers between devices: 87.8 us -> 52.7 us
  starting transfers between devices: 13.8 us -> 19.2 us
  local copies, waits for them, and re-layouts: 23.3 us -> 27.8 us
    psum x1, blocking collectives: 25 us -> 196 us  [body(): lax.psum((jnp.sum(filtered, axis=1), jnp.sum(filtered * filtered, axis=1)...]
    all_gather x1 -> x0, waiting for transfers between devices: 35.8 us -> none  [body(): lax.all_gather(expert_hidden, 'tp', axis=1, tiled=True)]
    all_to_all x0 -> x1, starting transfers between devices: none -> 4.88 us  [body(): lax.all_to_all(jnp.stack([s0 for _ in range(lax.psum(1, axis_name='tp'))]...]
    another operation x1 -> x2, local copies, waits for them, and re-layouts: 0.01 us -> 4.3 us  [the longest x1 4.29 us: body(): jnp.stack([s0 for _ in range(lax.psum(1, axis_name='tp'))])]
  transfers between devices with their start and end apart: 6 -> 6, of which waited for: 4 -> 3; matrix products, arithmetic and copies ran while one was open for 6% -> 4% of each run, Pallas kernels for 0% -> 0%
where the time goes in v1:
time: 373 us; the launch traced here: 372 us
  blocking collectives  237 us (64%)
  waiting for transfers between devices  52.7 us (14%)
  local copies, waits for them, and re-layouts  27.8 us (7%)
  starting transfers between devices  19.2 us (5%)
  between operations  14.3 us (4%)
  matrix products  13.7 us (4%)
  other arithmetic  6.99 us (2%)
    psum x1, blocking collectives, body(): lax.psum((jnp.sum(filtered, axis=1), jnp.sum(filtered * filtered, axis=1)...  196 us
    all_gather x1, waiting for transfers between devices, body(): arrived = lax.all_gather(partial_rows, 'tp', axis=1, tiled=True)  42.2 us
    all_to_all x1, blocking collectives, body(): lax.all_to_all(own_slots, EP, split_axis=0, concat_axis=0, tiled=True)  24.8 us
    all_gather x1, blocking collectives, body(): lax.all_gather(shared_hidden, 'tp', axis=1, tiled=True)  16.5 us
    scatter x1, local copies, waits for them, and re-layouts, body(): outgoing = jnp.zeros((groups * capacity, model_width), jnp.bfloat16).at[s...  12.8 us
    all_to_all x2, starting transfers between devices, exchange_in_order(): lax.all_to_all(parts, axes[k], split_axis=k, concat_axis=k, tiled=True)  11.2 us
    all_gather x1, waiting for transfers between devices, body(): lax.all_gather(conv_hidden, 'tp', axis=1, tiled=True)  9.75 us
  transfers between devices with their start and end apart: 6, of which 3 were waited for; matrix products, arithmetic and copies ran while one was open for 4% of the time, Pallas kernels for 0%

profile of v1, /device:TPU:1, one launch (start us, length us, event | category | flops | bytes accessed | tf_op | source)
XLA Modules:
  0.0 372.0 jit_solution(7749784929222617143)
XLA Ops:
  7.2 0.0 copy-start
  7.2 0.0 all-gather.5.cloned.1.call-start
  7.2 0.8 broadcast_multiply_fusion
  8.0 0.8 copy.35
  8.8 0.1 eq.29
  8.9 0.1 eq.25
  9.0 1.2 fusion.6
  10.3 0.1 copy.34
  10.4 0.1 mul.506
  10.5 1.2 reduce-window.6
  11.7 0.2 slice_reduce_fusion
  11.9 0.1 fusion.45
  12.1 1.2 fusion.8
  13.3 12.8 %scatter_custom_fusion = bf16[1024,2048]{1,0:T(8,128)(2,1)} fusion(s32[512]{0:T(512)S(1)} %bitcast.121, bf16[128,2048]{1,0:T(8,128)(2,1)S(1)} %fusion.8, s32[1024]{0:T(1024)S(1)} %pad_clamp_fusion.1, bf16[]{:T(256)} %constant.47.clone.1), kind=kCustom, calls=%fused_computation.3 | custom fusion | bytes 4194306 | tf_op jit(solution)/shard_map/scatter | solution.py:104
  26.1 1.5 constant_dynamic-slice_fusion
  27.6 24.8 %all_to_all.20 = bf16[32,2,2048]{2,1,0:T(2,128)(2,1)S(1)} all-to-all(bf16[32,2,2048]{2,1,0:T(2,128)(2,1)S(1)} %constant_dynamic-slice_fusion), channel_id=1, replica_groups=mesh['ep_0'=8,'ep_1'=4,'tp'=16] {'ep_0','ep_1'}, dimensions={0} | all-to-all | bytes 524288 | tf_op jit(solution)/shard_map/all_to_all | solution.py:109
  52.4 0.8 copy.38
  53.2 0.0 all-gather.5.cloned.1.call-update
  53.2 42.2 %all-gather.5.cloned.1.call-done = bf16[32,32,2048]{2,0,1:T(8,128)(2,1)} async-done(((bf16[32,2,2048]{2,0,1:T(8,128)(2,1)}), bf16[32,32,2048]{2,0,1:T(8,128)(2,1)}) %all-gather.5.cloned.1.call-update) | async-done | bytes 4194320 | tf_op jit(solution)/shard_map/all_gather | solution.py:110
  95.4 4.5 %copy.39 = bf16[32,32,2048]{2,1,0:T(8,128)(2,1)S(1)} copy(bf16[32,32,2048]{2,0,1:T(8,128)(2,1)} %all-gather.5.cloned.1.call-done) | data formatting | bytes 8388608 | tf_op jit(solution)/shard_map/all_gather | solution.py:110
  99.9 0.0 copy-start.11
  99.9 1.3 fusion.11
  101.2 1.3 fusion.3
  102.5 0.2 copy.40
  102.7 4.3 %stack.2 = bf16[16,1024,256]{1,2,0:T(8,128)(2,1)} broadcast(bf16[1024,256]{0,1:T(8,128)(2,1)S(1)} %copy.40), dimensions={1,2} | broadcast | bytes 8912896 | tf_op jit(solution)/shard_map/stack | solution.py:123
  107.0 4.9 %all-to-all-start.1 = ((bf16[16,1024,256]{1,2,0:T(8,128)(2,1)}), bf16[16,1024,256]{1,2,0:T(8,128)(2,1)}, u32[]{:S(2)}, u32[]{:S(2)}) async-start(bf16[16,1024,256]{1,2,0:T(8,128)(2,1)} %stack.2), calls=%async_computation.1 | async-start | bytes 16777216 | tf_op jit(solution)/shard_map/all_to_all | solution.py:122
  111.9 0.0 all-gather.3.cloned.1.call-start
  112.0 0.1 multiply_convert_fusion.1
  112.1 3.1 collective-permute-start
  115.2 0.7 collective-permute-done
  115.9 1.2 fusion.47
  117.1 195.9 %all-reduce = (f32[512]{0:T(512)S(1)}, f32[512]{0:T(512)S(1)}) all-reduce(f32[512]{0:T(512)S(1)} %get-tuple-element.3, f32[512]{0:T(512)S(1)} %get-tuple-element.2), channel_id=1, replica_groups=mesh['ep_0'=8,'ep_1'=4,'tp'=16] {'tp'}, use_global_device_ids=true, to_apply=%region_3.0 | all-reduce | flops 1024 | bytes 8192 | tf_op jit(solution)/shard_map/psum | solution.py:70
  313.1 0.9 multiply_convert_fusion
  314.0 0.0 all-gather.3.cloned.1.call-update
  314.1 6.8 %convolution_convert_fusion = bf16[1024,128]{1,0:T(8,128)(2,1)} fusion(bf16[1024,4096]{0,1:T(8,128)(2,1)} %bitcast.40, bf16[1,4096,128]{2,1,0:T(8,128)(2,1)} %param.28), kind=kOutput, calls=%fused_computation.39 | convolution fusion | flops 1073872896 | bytes 9699328 | tf_op jit(solution)/shard_map/dot_general | solution.py:130
  320.9 7.2 %all-to-all-start.2 = ((bf16[8,4,1,32,128]{4,3,1,2,0:T(8,128)(2,1)}), bf16[8,4,1,32,128]{4,3,1,2,0:T(8,128)(2,1)S(1)}, u32[]{:S(2)}, u32[]{:S(2)}) async-start(bf16[8,4,1,32,128]{4,3,1,2,0:T(8,128)(2,1)} %bitcast.43), calls=%async_computation.2 | async-start | bytes 524288 | tf_op jit(solution)/shard_map/all_to_all | solution.py:31
  328.1 0.3 fusion.48
  328.4 0.0 copy-done.8
  328.4 0.1 copy.44
  328.5 0.3 fusion.5
  328.8 16.5 %all_gather.11 = bf16[128,512]{0,1:T(8,128)(2,1)S(1)} all-gather(bf16[128,32]{0,1:T(8,128)(2,1)S(1)} %fusion.5), channel_id=1, replica_groups=mesh['ep_0'=8,'ep_1'=4,'tp'=16] {'tp'}, dimensions={1}, use_global_device_ids=true | all-gather | bytes 139264 | tf_op jit(solution)/shard_map/all_gather | solution.py:134
  345.3 0.7 copy.42
  346.0 4.0 %all-to-all-start.3 = ((bf16[8,4,1,32,128]{4,3,0,2,1:T(8,128)(2,1)}), bf16[8,4,1,32,128]{4,3,0,2,1:T(8,128)(2,1)S(1)}, u32[]{:S(2)}, u32[]{:S(2)}) async-start(bf16[8,4,1,32,128]{4,3,0,2,1:T(8,128)(2,1)} %copy.42), calls=%async_computation.3 | async-start | bytes 524288 | tf_op jit(solution)/shard_map/all_to_all | solution.py:31
  350.0 9.8 %all-gather.3.cloned.1.call-done = bf16[512,2048]{1,0:T(8,128)(2,1)} async-done(((bf16[512,128]{1,0:T(8,128)(2,1)}), bf16[512,2048]{1,0:T(8,128)(2,1)}) %all-gather.3.cloned.1.call-update) | async-done | bytes 2097168 | tf_op jit(solution)/shard_map/all_gather | solution.py:81
  359.7 3.0 convolution_convert_fusion.1
  362.7 1.3 gather_fusion
  364.1 0.2 fusion.13
  364.3 0.8 fusion.4
  (37 shorter events, 0.2 us)
Async XLA Ops:
  7.2 92.7 %copy-start = (bf16[1,2048,256]{2,1,0:T(8,128)(2,1)S(1)}, bf16[1,2048,256]{2,1,0:T(8,128)(2,1)}, u32[]{:S(2)}) copy-start(bf16[1,2048,256]{2,1,0:T(8,128)(2,1)} %param.26) | copy-start | bytes 3145732
  7.2 88.2 %all-gather.5.cloned.1.call-start = ((), (), s32[]{:S(2)}) async-start(), calls=%async_computation.5 | async-start | bytes 4456448 | tf_op jit(solution)/shard_map/all_gather | solution.py:110
  99.9 1.3 copy-start.11
  107.0 4.9 %copy-start.2 = (bf16[512,128]{1,0:T(8,128)(2,1)S(1)}, bf16[512,128]{1,0:T(8,128)(2,1)}, u32[]{:S(2)}) copy-start(bf16[512,128]{1,0:T(8,128)(2,1)} %param.17) | copy-start | bytes 393220
  107.0 5.0 %copy-start.3 = (bf16[512,128]{1,0:T(8,128)(2,1)S(1)}, bf16[512,128]{1,0:T(8,128)(2,1)}, u32[]{:S(2)}) copy-start(bf16[512,128]{1,0:T(8,128)(2,1)} %param.16) | copy-start | bytes 393220
  107.0 8.2 %copy-start.7 = (f32[31,128]{1,0:T(8,128)S(1)}, f32[31,128]{1,0:T(8,128)}, u32[]{:S(2)}) copy-start(f32[31,128]{1,0:T(8,128)} %param.18) | copy-start | bytes 47620
  107.0 206.1 %copy-start.9 = (f32[128]{0:T(128)S(1)}, f32[128]{0:T(128)}, u32[]{:S(2)}) copy-start(f32[128]{0:T(128)} %param.20) | copy-start | bytes 1540
  107.0 206.1 %copy-start.10 = (f32[128]{0:T(128)S(1)}, f32[128]{0:T(128)}, u32[]{:S(2)}) copy-start(f32[128]{0:T(128)} %param.19) | copy-start | bytes 1540
  107.0 207.0 %all-to-all-start.1 = ((bf16[16,1024,256]{1,2,0:T(8,128)(2,1)}), bf16[16,1024,256]{1,2,0:T(8,128)(2,1)}, u32[]{:S(2)}, u32[]{:S(2)}) async-start(bf16[16,1024,256]{1,2,0:T(8,128)(2,1)} %stack.2), calls=%async_computation.1 | async-start | bytes 16777216 | tf_op jit(solution)/shard_map/all_to_all | solution.py:122
  111.9 247.8 %all-gather.3.cloned.1.call-start = ((), (), s32[]{:S(2)}) async-start(), calls=%async_computation.4 | async-start | bytes 2228224 | tf_op jit(solution)/shard_map/all_gather | solution.py:81
  112.1 3.9 %collective-permute-start = (bf16[30,128]{1,0:T(8,128)(2,1)S(1)}, bf16[30,128]{1,0:T(8,128)(2,1)S(1)}, u32[]{:S(2)}, u32[]{:S(2)}) collective-permute-start(bf16[30,128]{1,0:T(8,128)(2,1)S(1)} %slice.260), channel_id=1, source_target_pairs={{0,16},{16,32},{32,48},{48,64},{64,80},{80,96},{96,112},{112,128},... | collective-permute-start | bytes 23048 | tf_op jit(solution)/shard_map/ppermute | solution.py:13
  314.0 14.1 %copy-start.4 = (bf16[2048,32]{0,1:T(8,128)(2,1)S(1)}, bf16[2048,32]{0,1:T(8,128)(2,1)}, u32[]{:S(2)}) copy-start(bf16[2048,32]{0,1:T(8,128)(2,1)} %param.29) | copy-start | bytes 393220
  314.0 14.4 %copy-start.8 = (f32[128,4]{0,1:T(4,128)S(1)}, f32[128,4]{0,1:T(4,128)}, u32[]{:S(2)}) copy-start(f32[128,4]{0,1:T(4,128)} %param.25) | copy-start | bytes 6148
  314.0 14.5 %copy-start.5 = (bf16[2048,32]{0,1:T(8,128)(2,1)S(1)}, bf16[2048,32]{0,1:T(8,128)(2,1)}, u32[]{:S(2)}) copy-start(bf16[2048,32]{0,1:T(8,128)(2,1)} %param.30) | copy-start | bytes 393220
  314.1 45.7 %copy-start.1 = (bf16[2048,128]{1,0:T(8,128)(2,1)S(1)}, bf16[2048,128]{1,0:T(8,128)(2,1)}, u32[]{:S(2)}) copy-start(bf16[2048,128]{1,0:T(8,128)(2,1)} %param.21) | copy-start | bytes 1572868
  320.9 43.5 %copy-start.6 = (bf16[512,128]{1,0:T(8,128)(2,1)S(1)}, bf16[512,128]{1,0:T(8,128)(2,1)}, u32[]{:S(2)}) copy-start(bf16[512,128]{1,0:T(8,128)(2,1)} %param.31) | copy-start | bytes 393220
  320.9 24.4 %all-to-all-start.2 = ((bf16[8,4,1,32,128]{4,3,1,2,0:T(8,128)(2,1)}), bf16[8,4,1,32,128]{4,3,1,2,0:T(8,128)(2,1)S(1)}, u32[]{:S(2)}, u32[]{:S(2)}) async-start(bf16[8,4,1,32,128]{4,3,1,2,0:T(8,128)(2,1)} %bitcast.43), calls=%async_computation.2 | async-start | bytes 524288 | tf_op jit(solution)/shard_map/all_to_all | solution.py:31
  346.0 16.7 %all-to-all-start.3 = ((bf16[8,4,1,32,128]{4,3,0,2,1:T(8,128)(2,1)}), bf16[8,4,1,32,128]{4,3,0,2,1:T(8,128)(2,1)S(1)}, u32[]{:S(2)}, u32[]{:S(2)}) async-start(bf16[8,4,1,32,128]{4,3,0,2,1:T(8,128)(2,1)} %copy.42), calls=%async_computation.3 | async-start | bytes 524288 | tf_op jit(solution)/shard_map/all_to_all | solution.py:31
Sparse Core Ops, SparseCore 0:
  53.3 42.0 all-gather.4
  314.1 45.5 all-gather.2
